TPU v7x, 32 devices: a whole 2x2x4 slice. The times are simulated.
32 devices in a mesh: fs: 8 (over z, x), tp: 4 (over y, core).
Axes of the slice: x: 2, y: 2, z: 4, core: 2. Of those that a mesh axis runs over, the one named last changes fastest.
Arguments:
- query_rows: bfloat16 [16384, 2048], P('fs', 'tp'), may hold values from -16 to 16
- key_rows: bfloat16 [16384, 2048], P('fs', 'tp'), may hold values from -8 to 8
- value_rows: bfloat16 [16384, 2048], P('fs', 'tp'), may hold values from -6 to 6
- mix_lambda: float32 [16], P('tp'), may hold values from 0.3 to 0.8
- head_gain: float32 [128], replicated, may hold values from 0.1 to 1.9
- out_cotangent: bfloat16 [16384, 2048], P('fs'), may hold values from -0.049804688 to 0.049804688
- layer_input: bfloat16 [16384, 2048], P('fs'), may hold values from -6 to 6
- value_cotangent: bfloat16 [16384, 2048], P('fs', 'tp'), may hold values from -0.049804688 to 0.049804688
- out_weight: float32 [2048, 2048], P('tp', 'fs'), may hold values from -0.125 to 0.125
- value_weight: float32 [2048, 2048], P('fs', 'tp'), may hold values from -0.125 to 0.125
- out_basis: bfloat16 [2048, 256], replicated, may hold values from -0.125 to 0.125
- value_basis: bfloat16 [2048, 256], replicated, may hold values from -0.125 to 0.125
- out_first: float32 [256, 2048], P('fs', 'tp'), may hold values from -20 to 20
- out_second: float32 [256, 2048], P('fs', 'tp'), may hold values from 0.02 to 0.5
- value_first: float32 [256, 2048], P('fs', 'tp'), may hold values from -20 to 20
- value_second: float32 [256, 2048], P('fs', 'tp'), may hold values from 0.02 to 0.5
Outputs:
- out_step: float32 [2048, 2048], P('tp', 'fs')
- value_step: float32 [2048, 2048], P('fs', 'tp')
- new_out_weight: float32 [2048, 2048], P('tp', 'fs')
- new_value_weight: float32 [2048, 2048], P('fs', 'tp')
- out_copy: bfloat16 [2048, 2048], P('tp')
- value_copy: bfloat16 [2048, 2048], P(None, 'tp')
- new_out_first: float32 [256, 2048], P('fs', 'tp')
- new_out_second: float32 [256, 2048], P('fs', 'tp')
- new_value_first: float32 [256, 2048], P('fs', 'tp')
- new_value_second: float32 [256, 2048], P('fs', 'tp')
All inputs are finite; a program needn't handle non-finite values.
Results may differ from a plain program's by a relative error of at most 0.001.
Values may be sent and summed in bfloat16 or wider, within the bound.
A program may use at most 192 MiB of HBM per device.

v0:
```python
import math

import jax
import jax.numpy as jnp
from jax import lax
from jax.sharding import PartitionSpec as P

DH = 64
DV = 128


EPSILON_NORM = 1e-05
EPSILON_ADAM = 1e-08
BETA_ONE = 0.9
BETA_TWO = 0.95
CLIP_RMS = 1.0
LEARN_RATE = 0.01


def attend_blocks(query_rows, key_rows, value_rows, mix_lambda, head_gain):
    seq_len = query_rows.shape[0]
    head_count = mix_lambda.shape[0]
    span_rows = min(512, seq_len)
    query_four = query_rows.reshape(seq_len, head_count, 2, DH)
    key_four = key_rows.reshape(seq_len, head_count, 2, DH)
    value_three = value_rows.reshape(seq_len, head_count, DV)
    key_pos = lax.iota(jnp.int32, seq_len)

    def one_block(block_index):
        row_start = block_index * span_rows
        query_block = lax.dynamic_slice_in_dim(query_four, row_start, span_rows, 0)
        scores = jnp.einsum(
            "qhmd,khmd->hmqk", query_block, key_four, preferred_element_type=jnp.float32
        ) * DH ** (-0.5)
        query_pos = row_start + lax.iota(jnp.int32, span_rows)
        causal = key_pos[None, :] <= query_pos[:, None]
        scores = jnp.where(causal, scores, -jnp.inf)
        row_peak = jnp.max(scores, axis=-1, keepdims=True)
        exp_scores = jnp.exp(scores - row_peak)
        soft_maps = exp_scores / jnp.sum(exp_scores, axis=-1, keepdims=True)
        mix_weights = (soft_maps[:, 0] - mix_lambda[:, None, None] * soft_maps[:, 1]).astype(
            jnp.bfloat16
        )
        raw_out = jnp.einsum(
            "hqk,khv->qhv", mix_weights, value_three, preferred_element_type=jnp.float32
        )
        normed = (
            raw_out
            * lax.rsqrt(jnp.mean(raw_out * raw_out, axis=-1, keepdims=True) + EPSILON_NORM)
            * head_gain
        )
        return normed.astype(jnp.bfloat16).reshape(span_rows, head_count * DV)

    blocks = lax.map(one_block, jnp.arange(seq_len // span_rows))
    return blocks.reshape(seq_len, head_count * DV)


def project_partial(partial_value, basis):
    basis_part = basis.astype(jnp.float32)
    return lax.psum_scatter(
        jnp.einsum("dr,dv->rv", basis_part, partial_value, precision=lax.Precision.HIGHEST),
        "fs",
        scatter_dimension=0,
        tiled=True,
    )


def moment_step(proj, first, second):
    new_first = BETA_ONE * first + (1.0 - BETA_ONE) * proj
    new_second = BETA_TWO * second + (1.0 - BETA_TWO) * proj * proj
    direction = new_first / (jnp.sqrt(new_second) + EPSILON_ADAM)
    return (new_first, new_second, direction)


def body(
    query_rows,
    key_rows,
    value_rows,
    mix_lambda,
    head_gain,
    out_cotangent,
    layer_input,
    value_cotangent,
    out_weight,
    value_weight,
    out_basis,
    value_basis,
    out_first,
    out_second,
    value_first,
    value_second,
):
    head_out = attend_blocks(query_rows, key_rows, value_rows, mix_lambda, head_gain)
    fs_count = lax.axis_size("fs")
    row_share = out_cotangent.shape[1] // fs_count
    row_base = lax.axis_index("fs") * row_share
    out_rows_b = lax.dynamic_slice_in_dim(out_basis, row_base, row_share, 0).astype(jnp.float32)
    value_rows_b = lax.dynamic_slice_in_dim(value_basis, row_base, row_share, 0).astype(jnp.float32)
    out_partial = jnp.einsum(
        "td,tv->dv", out_cotangent, head_out, preferred_element_type=jnp.float32
    )
    value_partial = jnp.einsum(
        "td,tv->dv", layer_input, value_cotangent, preferred_element_type=jnp.float32
    )
    out_proj = project_partial(out_partial, out_basis)
    value_proj = project_partial(value_partial, value_basis)
    new_out_first, new_out_second, out_dir = moment_step(out_proj, out_first, out_second)
    new_value_first, new_value_second, value_dir = moment_step(
        value_proj, value_first, value_second
    )
    out_sumsq, value_sumsq = lax.psum(
        (jnp.sum(out_dir * out_dir), jnp.sum(value_dir * value_dir)), ("fs", "tp")
    )
    entry_count = out_first.shape[0] * fs_count * out_first.shape[1] * lax.axis_size("tp")
    out_clip = jnp.minimum(1.0, CLIP_RMS * math.sqrt(entry_count) / jnp.sqrt(out_sumsq))
    value_clip = jnp.minimum(1.0, CLIP_RMS * math.sqrt(entry_count) / jnp.sqrt(value_sumsq))
    out_total = jnp.dot(
        out_rows_b,
        lax.all_gather(out_dir, "fs", axis=0, tiled=True),
        precision=lax.Precision.HIGHEST,
    )
    value_total = jnp.dot(
        value_rows_b,
        lax.all_gather(value_dir, "fs", axis=0, tiled=True),
        precision=lax.Precision.HIGHEST,
    )
    value_step = value_clip * value_total
    out_step = (out_clip * out_total).T
    new_value_weight = value_weight - LEARN_RATE * value_step
    new_out_weight = out_weight - LEARN_RATE * out_step
    out_copy, value_copy = (
        lax.all_gather(new_out_weight.astype(jnp.bfloat16), "fs", axis=1, tiled=True),
        lax.all_gather(new_value_weight.astype(jnp.bfloat16), "fs", axis=0, tiled=True),
    )
    return (
        out_step,
        value_step,
        new_out_weight,
        new_value_weight,
        out_copy,
        value_copy,
        new_out_first,
        new_out_second,
        new_value_first,
        new_value_second,
    )


def solution(mesh):
    placed = (
        P("fs", "tp"),
        P("fs", "tp"),
        P("fs", "tp"),
        P("tp"),
        P(),
        P("fs", None),
        P("fs", None),
        P("fs", "tp"),
        P("tp", "fs"),
        P("fs", "tp"),
        P(),
        P(),
        P("fs", "tp"),
        P("fs", "tp"),
        P("fs", "tp"),
        P("fs", "tp"),
    )
    return jax.shard_map(
        body,
        mesh=mesh,
        in_specs=placed,
        out_specs=(
            P("tp", "fs"),
            P("fs", "tp"),
            P("tp", "fs"),
            P("fs", "tp"),
            P("tp", None),
            P(None, "tp"),
            P("fs", "tp"),
            P("fs", "tp"),
            P("fs", "tp"),
            P("fs", "tp"),
        ),
        check_vma=False,
    )
```

profile of v0, /device:TPU:0, one launch (start us, length us, event | category | flops | bytes accessed | tf_op | source)
XLA Modules:
  0.0 579.0 jit_solution(7291972011320459516)
XLA Ops:
  7.2 4.1 copy.67
  11.3 4.0 copy.68
  19.3 228.3 %while.11 = (s32[]{:T(128)}, bf16[4,512,512]{2,1,0:T(8,128)(2,1)}, s32[4]{0:T(128)S(1)}, bf16[2048,4,2,64]{0,3,2,1:T(8,128)(2,1)}, bf16[2048,4,2,64]{0,3,2,1:T(8...) while((s32[]{:T(128)}, bf16[4,512,512]{2,1,0:T(8,128)(2,1)}, ...), condition=%wide.region_4.5_spmd.clone, body=%wide.region_0.4_spmd.clone.sunk | while | flops 2204373504 | bytes 154211568 | solution.py:54
  21.2 17.9 %fusion.67 = (f32[4,2,512]{2,1,0:T(2,128)S(1)}, f32[4,2,512,2048]{3,2,1,0:T(8,128)}) fusion(pred[512,2048]{1,0:T(8,128)(4,1)S(1)} %iota_compare_fusion.2, bf16[2048,4,2,64]{0,3,2,1:T(8,128)(2,1)} %get-tuple-element.227, bf16[2048,4,2,64]{0,3,2,1:T(8,128)(2,1)} %get-tuple-element.226, s32[]{:T(128)S(6)} %select_n.27), kind=kOutput, calls=%fused_computation.52.clone.1 | convolution fusion | flops 1107298304 | bytes 37240836 | tf_op jit(solution)/shard_map/while/body/eval_jaxpr/sub | solution.py:39
  39.1 23.7 %broadcast_divide_fusion.2 = f32[4,2,512,2048]{3,2,1,0:T(8,128)} fusion(f32[4,2,512,2048]{3,2,1,0:T(8,128)} %get-tuple-element.195, f32[4,2,512]{2,1,0:T(2,128)S(1)} %get-tuple-element.196), kind=kLoop, calls=%fused_computation.10.clone.1 | loop fusion | flops 8388608 | bytes 67125248 | tf_op jit(solution)/shard_map/while/body/eval_jaxpr/div | solution.py:40
  62.9 12.3 %multiply_reduce_fusion.4 = (f32[512,4]{0,1:T(4,128)S(1)}, f32[512,4,128]{0,2,1:T(8,128)S(1)}) fusion(bf16[2048,4,128]{0,2,1:T(8,128)(2,1)S(1)} %copy-done.1, f32[4,2,512,2048]{3,2,1,0:T(8,128)} %broadcast_divide_fusion.2, f32[4]{0:T(128)S(1)} %get-tuple-element.228), kind=kOutput, calls=%fused_computation.19.clone.1 | convolution fusion | flops 1086846976 | bytes 36708368 | tf_op jit(solution)/shard_map/while/body/eval_jaxpr/hqk,khv->qhv/dot_general | solution.py:44
  78.3 17.9 %fusion.67 = (f32[4,2,512]{2,1,0:T(2,128)S(1)}, f32[4,2,512,2048]{3,2,1,0:T(8,128)}) fusion(pred[512,2048]{1,0:T(8,128)(4,1)S(1)} %iota_compare_fusion.2, bf16[2048,4,2,64]{0,3,2,1:T(8,128)(2,1)} %get-tuple-element.227, bf16[2048,4,2,64]{0,3,2,1:T(8,128)(2,1)} %get-tuple-element.226, s32[]{:T(128)S(6)} %select_n.27), kind=kOutput, calls=%fused_computation.52.clone.1 | convolution fusion | flops 1107298304 | bytes 37240836 | tf_op jit(solution)/shard_map/while/body/eval_jaxpr/sub | solution.py:39
  96.2 23.7 %broadcast_divide_fusion.2 = f32[4,2,512,2048]{3,2,1,0:T(8,128)} fusion(f32[4,2,512,2048]{3,2,1,0:T(8,128)} %get-tuple-element.195, f32[4,2,512]{2,1,0:T(2,128)S(1)} %get-tuple-element.196), kind=kLoop, calls=%fused_computation.10.clone.1 | loop fusion | flops 8388608 | bytes 67125248 | tf_op jit(solution)/shard_map/while/body/eval_jaxpr/div | solution.py:40
  119.9 12.3 %multiply_reduce_fusion.4 = (f32[512,4]{0,1:T(4,128)S(1)}, f32[512,4,128]{0,2,1:T(8,128)S(1)}) fusion(bf16[2048,4,128]{0,2,1:T(8,128)(2,1)S(1)} %copy-done.1, f32[4,2,512,2048]{3,2,1,0:T(8,128)} %broadcast_divide_fusion.2, f32[4]{0:T(128)S(1)} %get-tuple-element.228), kind=kOutput, calls=%fused_computation.19.clone.1 | convolution fusion | flops 1086846976 | bytes 36708368 | tf_op jit(solution)/shard_map/while/body/eval_jaxpr/hqk,khv->qhv/dot_general | solution.py:44
  135.4 17.9 %fusion.67 = (f32[4,2,512]{2,1,0:T(2,128)S(1)}, f32[4,2,512,2048]{3,2,1,0:T(8,128)}) fusion(pred[512,2048]{1,0:T(8,128)(4,1)S(1)} %iota_compare_fusion.2, bf16[2048,4,2,64]{0,3,2,1:T(8,128)(2,1)} %get-tuple-element.227, bf16[2048,4,2,64]{0,3,2,1:T(8,128)(2,1)} %get-tuple-element.226, s32[]{:T(128)S(6)} %select_n.27), kind=kOutput, calls=%fused_computation.52.clone.1 | convolution fusion | flops 1107298304 | bytes 37240836 | tf_op jit(solution)/shard_map/while/body/eval_jaxpr/sub | solution.py:39
  153.3 23.7 %broadcast_divide_fusion.2 = f32[4,2,512,2048]{3,2,1,0:T(8,128)} fusion(f32[4,2,512,2048]{3,2,1,0:T(8,128)} %get-tuple-element.195, f32[4,2,512]{2,1,0:T(2,128)S(1)} %get-tuple-element.196), kind=kLoop, calls=%fused_computation.10.clone.1 | loop fusion | flops 8388608 | bytes 67125248 | tf_op jit(solution)/shard_map/while/body/eval_jaxpr/div | solution.py:40
  177.0 12.3 %multiply_reduce_fusion.4 = (f32[512,4]{0,1:T(4,128)S(1)}, f32[512,4,128]{0,2,1:T(8,128)S(1)}) fusion(bf16[2048,4,128]{0,2,1:T(8,128)(2,1)S(1)} %copy-done.1, f32[4,2,512,2048]{3,2,1,0:T(8,128)} %broadcast_divide_fusion.2, f32[4]{0:T(128)S(1)} %get-tuple-element.228), kind=kOutput, calls=%fused_computation.19.clone.1 | convolution fusion | flops 1086846976 | bytes 36708368 | tf_op jit(solution)/shard_map/while/body/eval_jaxpr/hqk,khv->qhv/dot_general | solution.py:44
  192.4 17.9 %fusion.67 = (f32[4,2,512]{2,1,0:T(2,128)S(1)}, f32[4,2,512,2048]{3,2,1,0:T(8,128)}) fusion(pred[512,2048]{1,0:T(8,128)(4,1)S(1)} %iota_compare_fusion.2, bf16[2048,4,2,64]{0,3,2,1:T(8,128)(2,1)} %get-tuple-element.227, bf16[2048,4,2,64]{0,3,2,1:T(8,128)(2,1)} %get-tuple-element.226, s32[]{:T(128)S(6)} %select_n.27), kind=kOutput, calls=%fused_computation.52.clone.1 | convolution fusion | flops 1107298304 | bytes 37240836 | tf_op jit(solution)/shard_map/while/body/eval_jaxpr/sub | solution.py:39
  210.4 23.7 %broadcast_divide_fusion.2 = f32[4,2,512,2048]{3,2,1,0:T(8,128)} fusion(f32[4,2,512,2048]{3,2,1,0:T(8,128)} %get-tuple-element.195, f32[4,2,512]{2,1,0:T(2,128)S(1)} %get-tuple-element.196), kind=kLoop, calls=%fused_computation.10.clone.1 | loop fusion | flops 8388608 | bytes 67125248 | tf_op jit(solution)/shard_map/while/body/eval_jaxpr/div | solution.py:40
  234.1 12.3 %multiply_reduce_fusion.4 = (f32[512,4]{0,1:T(4,128)S(1)}, f32[512,4,128]{0,2,1:T(8,128)S(1)}) fusion(bf16[2048,4,128]{0,2,1:T(8,128)(2,1)S(1)} %copy-done.1, f32[4,2,512,2048]{3,2,1,0:T(8,128)} %broadcast_divide_fusion.2, f32[4]{0:T(128)S(1)} %get-tuple-element.228), kind=kOutput, calls=%fused_computation.19.clone.1 | convolution fusion | flops 1086846976 | bytes 36708368 | tf_op jit(solution)/shard_map/while/body/eval_jaxpr/hqk,khv->qhv/dot_general | solution.py:44
  247.6 7.8 %fusion.45 = f32[512,2048]{1,0:T(8,128)S(1)} fusion(bf16[2048,512]{1,0:T(8,128)(2,1)} %bitcast.67, bf16[2048,2048]{1,0:T(8,128)(2,1)} %param.23), kind=kOutput, calls=%fused_computation.53 | convolution fusion | flops 4294967296 | bytes 14680064 | tf_op jit(solution)/shard_map/td,tv->dv/dot_general | solution.py:99
  258.6 7.0 %fusion.46 = f32[2048,512]{1,0:T(8,128)S(1)} fusion(bf16[2048,2048]{1,0:T(8,128)(2,1)} %param.24, bf16[2048,512]{1,0:T(8,128)(2,1)S(1)} %copy-done), kind=kOutput, calls=%fused_computation.54 | convolution fusion | flops 4294967296 | bytes 14680064 | tf_op jit(solution)/shard_map/td,tv->dv/dot_general | solution.py:102
  270.2 53.8 %reduce-scatter.7.cloned.1.call-done = f32[32,512]{1,0:T(8,128)} async-done(((f32[256,512]{1,0:T(8,128)}), f32[32,512]{1,0:T(8,128)}) %reduce-scatter.7.cloned.1.call-update) | async-done | bytes 65552 | tf_op jit(solution)/shard_map/reduce_scatter | solution.py:60
  326.1 63.4 %reduce-scatter.9.cloned.1.call-done = f32[32,512]{1,0:T(8,128)} async-done(((f32[256,512]{1,0:T(8,128)}), f32[32,512]{1,0:T(8,128)}) %reduce-scatter.9.cloned.1.call-update) | async-done | bytes 65552 | tf_op jit(solution)/shard_map/reduce_scatter | solution.py:60
  391.6 40.2 %all-reduce = (f32[]{:T(128)}, f32[]{:T(128)}) all-reduce(f32[]{:T(128)} %get-tuple-element.132, f32[]{:T(128)} %get-tuple-element.128), channel_id=1, replica_groups=mesh['fs'=8,'tp'=4] {'fs','tp'}, use_global_device_ids=true, to_apply=%region_7.8 | all-reduce | flops 2 | bytes 16 | tf_op jit(solution)/shard_map/psum | solution.py:111
  432.5 31.4 %all_gather.13 = f32[256,512]{1,0:T(8,128)S(1)} all-gather(f32[32,512]{1,0:T(8,128)S(1)} %get-tuple-element.129), channel_id=1, replica_groups=mesh['fs'=8,'tp'=4] {'fs'}, dimensions={0}, use_global_device_ids=true | all-gather | bytes 589824 | tf_op jit(solution)/shard_map/all_gather | solution.py:124
  467.1 32.5 %all_gather.12 = f32[256,512]{1,0:T(8,128)S(1)} all-gather(f32[32,512]{1,0:T(8,128)S(1)} %get-tuple-element.133), channel_id=1, replica_groups=mesh['fs'=8,'tp'=4] {'fs'}, dimensions={0}, use_global_device_ids=true | all-gather | bytes 589824 | tf_op jit(solution)/shard_map/all_gather | solution.py:119
  502.3 13.6 %all-gather.5.cloned.1.call-done = bf16[2048,512]{1,0:T(8,128)(2,1)} async-done(((bf16[256,512]{1,0:T(8,128)(2,1)}), bf16[2048,512]{1,0:T(8,128)(2,1)}) %all-gather.5.cloned.1.call-update) | async-done | bytes 2097168 | tf_op jit(solution)/shard_map/all_gather | solution.py:133
  515.9 52.0 %all-gather.3.cloned.1.call-done = bf16[512,2048]{1,0:T(8,128)(2,1)} async-done(((bf16[512,256]{1,0:T(8,128)(2,1)}), bf16[512,2048]{1,0:T(8,128)(2,1)}) %all-gather.3.cloned.1.call-update) | async-done | bytes 2097168 | tf_op jit(solution)/shard_map/all_gather | solution.py:132
  (79 shorter events, 35.5 us)
Async XLA Ops:
  7.2 251.4 %copy-start = (bf16[2048,512]{1,0:T(8,128)(2,1)S(1)}, bf16[2048,512]{1,0:T(8,128)(2,1)}, u32[]{:S(2)}) copy-start(bf16[2048,512]{1,0:T(8,128)(2,1)} %param.25) | copy-start | bytes 6291460
  7.2 316.8 %reduce-scatter.7.cloned.1.call-start = ((), (), s32[]{:S(2)}) async-start(), calls=%async_computation.4 | async-start | bytes 589824 | tf_op jit(solution)/shard_map/reduce_scatter | solution.py:60
  11.3 8.0 %copy-start.10 = (f32[128]{0:T(128)S(1)}, f32[128]{0:T(128)}, u32[]{:S(2)}) copy-start(f32[128]{0:T(128)} %param.22) | copy-start | bytes 1540
  11.3 8.0 %copy-start.11 = (f32[4]{0:T(128)S(1)}, f32[4]{0:T(128)}, u32[]{:S(2)}) copy-start(f32[4]{0:T(128)} %param.21) | copy-start | bytes 52
  39.1 23.7 %copy-start.1 = (bf16[2048,4,128]{0,2,1:T(8,128)(2,1)S(1)}, bf16[2048,4,128]{0,2,1:T(8,128)(2,1)}, u32[]{:S(2)}) copy-start(bf16[2048,4,128]{0,2,1:T(8,128)(2,1)} %get-tuple-element.229) | copy-start | bytes 6291460 | tf_op jit(solution)/shard_map/while
  96.2 23.7 %copy-start.1 = (bf16[2048,4,128]{0,2,1:T(8,128)(2,1)S(1)}, bf16[2048,4,128]{0,2,1:T(8,128)(2,1)}, u32[]{:S(2)}) copy-start(bf16[2048,4,128]{0,2,1:T(8,128)(2,1)} %get-tuple-element.229) | copy-start | bytes 6291460 | tf_op jit(solution)/shard_map/while
  153.3 23.7 %copy-start.1 = (bf16[2048,4,128]{0,2,1:T(8,128)(2,1)S(1)}, bf16[2048,4,128]{0,2,1:T(8,128)(2,1)}, u32[]{:S(2)}) copy-start(bf16[2048,4,128]{0,2,1:T(8,128)(2,1)} %get-tuple-element.229) | copy-start | bytes 6291460 | tf_op jit(solution)/shard_map/while
  210.4 23.7 %copy-start.1 = (bf16[2048,4,128]{0,2,1:T(8,128)(2,1)S(1)}, bf16[2048,4,128]{0,2,1:T(8,128)(2,1)}, u32[]{:S(2)}) copy-start(bf16[2048,4,128]{0,2,1:T(8,128)(2,1)} %get-tuple-element.229) | copy-start | bytes 6291460 | tf_op jit(solution)/shard_map/while
  247.6 7.9 %copy-start.3 = (bf16[2048,256]{1,0:T(8,128)(2,1)S(1)}, bf16[2048,256]{1,0:T(8,128)(2,1)}, u32[]{:S(2)}) copy-start(bf16[2048,256]{1,0:T(8,128)(2,1)} %param.28) | copy-start | bytes 3145732
  258.5 130.9 %reduce-scatter.9.cloned.1.call-start = ((), (), s32[]{:S(2)}) async-start(), calls=%async_computation.5 | async-start | bytes 589824 | tf_op jit(solution)/shard_map/reduce_scatter | solution.py:60
  258.6 7.0 %copy-start.4 = (bf16[2048,256]{1,0:T(8,128)(2,1)S(1)}, bf16[2048,256]{1,0:T(8,128)(2,1)}, u32[]{:S(2)}) copy-start(bf16[2048,256]{1,0:T(8,128)(2,1)} %param.29) | copy-start | bytes 3145732
  265.6 58.3 %copy-start.6 = (f32[32,512]{1,0:T(8,128)S(1)}, f32[32,512]{1,0:T(8,128)}, u32[]{:S(2)}) copy-start(f32[32,512]{1,0:T(8,128)} %param.31) | copy-start | bytes 196612
  265.6 58.3 %copy-start.7 = (f32[32,512]{1,0:T(8,128)S(1)}, f32[32,512]{1,0:T(8,128)}, u32[]{:S(2)}) copy-start(f32[32,512]{1,0:T(8,128)} %param.30) | copy-start | bytes 196612
  265.6 123.8 %copy-start.8 = (f32[32,512]{1,0:T(8,128)S(1)}, f32[32,512]{1,0:T(8,128)}, u32[]{:S(2)}) copy-start(f32[32,512]{1,0:T(8,128)} %param.33) | copy-start | bytes 196612
  265.7 123.8 %copy-start.9 = (f32[32,512]{1,0:T(8,128)S(1)}, f32[32,512]{1,0:T(8,128)}, u32[]{:S(2)}) copy-start(f32[32,512]{1,0:T(8,128)} %param.32) | copy-start | bytes 196612
  265.7 198.2 %copy-start.5 = (f32[256,512]{1,0:T(8,128)S(1)}, f32[256,512]{1,0:T(8,128)}, u32[]{:S(2)}) copy-start(f32[256,512]{1,0:T(8,128)} %param.27) | copy-start | bytes 1572868
  270.1 245.8 %all-gather.5.cloned.1.call-start = ((), (), s32[]{:S(2)}) async-start(), calls=%async_computation.3 | async-start | bytes 2359296 | tf_op jit(solution)/shard_map/all_gather | solution.py:133
  466.3 101.5 %all-gather.3.cloned.1.call-start = ((), (), s32[]{:S(2)}) async-start(), calls=%async_computation.2 | async-start | bytes 2359296 | tf_op jit(solution)/shard_map/all_gather | solution.py:132
  567.8 3.3 copy-start.2
Sparse Core Ops, SparseCore 0:
  258.6 65.2 reduce-scatter.6
  327.9 61.5 reduce-scatter.8
  466.4 49.4 all-gather.4
  518.4 49.4 all-gather.2
where the time goes:
time: 580 us; the launch traced here: 579 us
  waiting for transfers between devices  183 us (32%)
  matrix products  146 us (25%)
  blocking collectives  104 us (18%)
  other arithmetic  102 us (18%)
  local copies, waits for them, and re-layouts  25.2 us (4%)
  between operations  15.3 us (3%)
    reduce_scatter x2, waiting for transfers between devices, project_partial(): lax.psum_scatter(jnp.einsum('dr,dv->rv', basis_part, partial_value, preci...  117 us
    div x4, other arithmetic, one_block(): soft_maps = exp_scores / jnp.sum(exp_scores, axis=-1, keepdims=True)  94.9 us
    sub x4, matrix products, one_block(): exp_scores = jnp.exp(scores - row_peak)  71.7 us
    all_gather x1, waiting for transfers between devices, body(): lax.all_gather(new_out_weight.astype(jnp.bfloat16), 'fs', axis=1, tiled=T...  52 us
    dot_general x4, matrix products, one_block(): jnp.einsum('hqk,khv->qhv', mix_weights, value_three, preferred_element_ty...  49.2 us
    psum x1, blocking collectives, body(): lax.psum((jnp.sum(out_dir * out_dir), jnp.sum(value_dir * value_dir)), ('...  40.2 us
    all_gather x1, blocking collectives, body(): lax.all_gather(out_dir, 'fs', axis=0, tiled=True)  32.5 us
    all_gather x1, blocking collectives, body(): lax.all_gather(value_dir, 'fs', axis=0, tiled=True)  31.4 us
  transfers between devices with their start and end apart: 4, of which 4 were waited for; matrix products, arithmetic and copies ran while one was open for 3% of the time, Pallas kernels for 0%

commit v1 on v0

--- a/solution.py
+++ b/solution.py
@@ -1,8 +1,11 @@
+import functools
 import math
 
 import jax
 import jax.numpy as jnp
 from jax import lax
+from jax.experimental import pallas as pl
+from jax.experimental.pallas import tpu as pltpu
 from jax.sharding import PartitionSpec as P
 
 DH = 64
@@ -15,53 +18,166 @@
 BETA_TWO = 0.95
 CLIP_RMS = 1.0
 LEARN_RATE = 0.01
-
-
-def attend_blocks(query_rows, key_rows, value_rows, mix_lambda, head_gain):
-    seq_len = query_rows.shape[0]
-    head_count = mix_lambda.shape[0]
-    span_rows = min(512, seq_len)
-    query_four = query_rows.reshape(seq_len, head_count, 2, DH)
-    key_four = key_rows.reshape(seq_len, head_count, 2, DH)
-    value_three = value_rows.reshape(seq_len, head_count, DV)
-    key_pos = lax.iota(jnp.int32, seq_len)
-
-    def one_block(block_index):
-        row_start = block_index * span_rows
-        query_block = lax.dynamic_slice_in_dim(query_four, row_start, span_rows, 0)
-        scores = jnp.einsum(
-            "qhmd,khmd->hmqk", query_block, key_four, preferred_element_type=jnp.float32
-        ) * DH ** (-0.5)
-        query_pos = row_start + lax.iota(jnp.int32, span_rows)
-        causal = key_pos[None, :] <= query_pos[:, None]
-        scores = jnp.where(causal, scores, -jnp.inf)
-        row_peak = jnp.max(scores, axis=-1, keepdims=True)
-        exp_scores = jnp.exp(scores - row_peak)
-        soft_maps = exp_scores / jnp.sum(exp_scores, axis=-1, keepdims=True)
-        mix_weights = (soft_maps[:, 0] - mix_lambda[:, None, None] * soft_maps[:, 1]).astype(
-            jnp.bfloat16
+TILE = 256
+F32 = jnp.float32
+BF16 = jnp.bfloat16
+
+
+def dot_f32(left, right, dims=((1,), (0,))):
+    return lax.dot_general(left, right, (dims, ((), ())), preferred_element_type=F32)
+
+
+def split_two(wide):
+    high = wide.astype(BF16)
+    return high, (wide - high.astype(F32)).astype(BF16)
+
+
+def fold_rows(tile, op):
+    rows, cols = tile.shape
+    return op(tile.reshape(rows // 8, 8, cols), axis=0)
+
+
+def grads_kernel(
+    lam_ref, query_ref, key_ref, value_ref, gain_ref, cot_ref, input_ref, vcot_ref,
+    obasis_ref, vbasis_ref, oproj_ref, vproj_ref,
+    score_one, score_two, mix_ref, value_t, obasis_t, vbasis_t, cb_high, cb_low,
+):
+    block = pl.program_id(0)
+    head = pl.program_id(1)
+    span = query_ref.shape[0]
+    seq_len = key_ref.shape[0]
+
+    @pl.when((block == 0) & (head == 0))
+    def _():
+        obasis_t[...] = obasis_ref[...].T
+        vbasis_t[...] = vbasis_ref[...].T
+        oproj_ref[...] = jnp.zeros_like(oproj_ref)
+        vproj_ref[...] = jnp.zeros_like(vproj_ref)
+
+    @pl.when(block == 0)
+    def _():
+        value_t[head] = value_ref[:, pl.ds(pl.multiple_of(head * DV, DV), DV)].T
+
+    @pl.when(head == 0)
+    def _():
+        cb = dot_f32(obasis_t[...], cot_ref[...], ((1,), (1,)))
+        high, low = split_two(cb)
+        cb_high[...] = high
+        cb_low[...] = low
+        high, low = split_two(dot_f32(vbasis_t[...], input_ref[...], ((1,), (1,))))
+        vcot = vcot_ref[...]
+        vproj_ref[...] += dot_f32(high, vcot) + dot_f32(low, vcot)
+
+    columns = pl.ds(pl.multiple_of(head * DV, DV), DV)
+    lam = lam_ref[head]
+    lane = lax.broadcasted_iota(jnp.int32, (span, DV), 1)
+    query = query_ref[:, columns].astype(F32) * DH ** (-0.5)
+    query_one = jnp.where(lane < DH, query, 0.0).astype(BF16)
+    query_two = jnp.where(lane < DH, 0.0, query).astype(BF16)
+
+    def attend(width, open_from):
+        def tiles():
+            return range(0, width, TILE)
+
+        peak_one = jnp.full((8, span), -jnp.inf, F32)
+        peak_two = peak_one
+        for at in tiles():
+            keys = key_ref[at : at + TILE, columns]
+            one = dot_f32(keys, query_one, ((1,), (1,)))
+            two = dot_f32(keys, query_two, ((1,), (1,)))
+            if at >= open_from:
+                key_pos = at + lax.broadcasted_iota(jnp.int32, (TILE, span), 0)
+                query_pos = block * span + lax.broadcasted_iota(jnp.int32, (TILE, span), 1)
+                causal = key_pos <= query_pos
+                one = jnp.where(causal, one, -jnp.inf)
+                two = jnp.where(causal, two, -jnp.inf)
+            score_one[at : at + TILE, :] = one
+            score_two[at : at + TILE, :] = two
+            peak_one = jnp.maximum(peak_one, fold_rows(one, jnp.max))
+            peak_two = jnp.maximum(peak_two, fold_rows(two, jnp.max))
+        peak_one = jnp.max(peak_one, axis=0, keepdims=True)
+        peak_two = jnp.max(peak_two, axis=0, keepdims=True)
+        sum_one = jnp.zeros((8, span), F32)
+        sum_two = sum_one
+        for at in tiles():
+            one = jnp.exp(score_one[at : at + TILE, :] - peak_one)
+            two = jnp.exp(score_two[at : at + TILE, :] - peak_two)
+            score_one[at : at + TILE, :] = one
+            score_two[at : at + TILE, :] = two
+            sum_one += fold_rows(one, jnp.sum)
+            sum_two += fold_rows(two, jnp.sum)
+        rate_one = 1.0 / jnp.sum(sum_one, axis=0, keepdims=True)
+        rate_two = lam / jnp.sum(sum_two, axis=0, keepdims=True)
+        for at in tiles():
+            mix_ref[at : at + TILE, :] = (
+                score_one[at : at + TILE, :] * rate_one - score_two[at : at + TILE, :] * rate_two
+            ).astype(BF16)
+        raw = dot_f32(value_t[head, :, :width], mix_ref[:width, :])
+        mean_sq = jnp.mean(raw * raw, axis=0, keepdims=True)
+        out_t = (raw * lax.rsqrt(mean_sq + EPSILON_NORM) * gain_ref[...]).astype(BF16)
+        oproj_ref[:, columns] += dot_f32(cb_high[...], out_t, ((1,), (1,))) + dot_f32(
+            cb_low[...], out_t, ((1,), (1,))
         )
-        raw_out = jnp.einsum(
-            "hqk,khv->qhv", mix_weights, value_three, preferred_element_type=jnp.float32
-        )
-        normed = (
-            raw_out
-            * lax.rsqrt(jnp.mean(raw_out * raw_out, axis=-1, keepdims=True) + EPSILON_NORM)
-            * head_gain
-        )
-        return normed.astype(jnp.bfloat16).reshape(span_rows, head_count * DV)
-
-    blocks = lax.map(one_block, jnp.arange(seq_len // span_rows))
-    return blocks.reshape(seq_len, head_count * DV)
-
-
-def project_partial(partial_value, basis):
-    basis_part = basis.astype(jnp.float32)
-    return lax.psum_scatter(
-        jnp.einsum("dr,dv->rv", basis_part, partial_value, precision=lax.Precision.HIGHEST),
-        "fs",
-        scatter_dimension=0,
-        tiled=True,
+
+    step = min(2 * span, seq_len)
+    for width in range(step, seq_len + 1, step):
+        lowest = (width - step) // span
+
+        @pl.when((block >= lowest) & (block < width // span))
+        def _(width=width):
+            attend(width, width - step)
+
+
+def local_grads(
+    query_rows, key_rows, value_rows, mix_lambda, head_gain, out_cotangent, layer_input,
+    value_cotangent, out_basis, value_basis,
+):
+    seq_len, cols = query_rows.shape
+    heads = mix_lambda.shape[0]
+    width = out_cotangent.shape[1]
+    rank = out_basis.shape[1]
+    span = min(TILE, seq_len)
+    blocks = seq_len // span
+    rows_spec = lambda wide: pl.BlockSpec((span, wide), lambda i, h: (i, 0))
+    whole = lambda a, b: pl.BlockSpec((a, b), lambda i, h: (0, 0))
+    return pl.pallas_call(
+        grads_kernel,
+        grid=(blocks, heads),
+        out_shape=(
+            jax.ShapeDtypeStruct((rank, cols), F32),
+            jax.ShapeDtypeStruct((rank, cols), F32),
+        ),
+        in_specs=[
+            pl.BlockSpec(memory_space=pltpu.SMEM),
+            rows_spec(cols),
+            whole(seq_len, cols),
+            whole(seq_len, cols),
+            whole(DV, 1),
+            rows_spec(width),
+            rows_spec(width),
+            rows_spec(cols),
+            whole(width, rank),
+            whole(width, rank),
+        ],
+        out_specs=(whole(rank, cols), whole(rank, cols)),
+        scratch_shapes=[
+            pltpu.VMEM((seq_len, span), F32),
+            pltpu.VMEM((seq_len, span), F32),
+            pltpu.VMEM((seq_len, span), BF16),
+            pltpu.VMEM((heads, DV, seq_len), BF16),
+            pltpu.VMEM((rank, width), BF16),
+            pltpu.VMEM((rank, width), BF16),
+            pltpu.VMEM((rank, span), BF16),
+            pltpu.VMEM((rank, span), BF16),
+        ],
+        compiler_params=pltpu.CompilerParams(
+            dimension_semantics=("arbitrary", "arbitrary"),
+            vmem_limit_bytes=60 * 1024 * 1024,
+        ),
+        name="grads",
+    )(
+        mix_lambda, query_rows, key_rows, value_rows, head_gain.reshape(DV, 1),
+        out_cotangent, layer_input, value_cotangent, out_basis, value_basis,
     )
 
 
@@ -90,20 +206,17 @@
     value_first,
     value_second,
 ):
-    head_out = attend_blocks(query_rows, key_rows, value_rows, mix_lambda, head_gain)
     fs_count = lax.axis_size("fs")
     row_share = out_cotangent.shape[1] // fs_count
     row_base = lax.axis_index("fs") * row_share
     out_rows_b = lax.dynamic_slice_in_dim(out_basis, row_base, row_share, 0).astype(jnp.float32)
     value_rows_b = lax.dynamic_slice_in_dim(value_basis, row_base, row_share, 0).astype(jnp.float32)
-    out_partial = jnp.einsum(
-        "td,tv->dv", out_cotangent, head_out, preferred_element_type=jnp.float32
-    )
-    value_partial = jnp.einsum(
-        "td,tv->dv", layer_input, value_cotangent, preferred_element_type=jnp.float32
-    )
-    out_proj = project_partial(out_partial, out_basis)
-    value_proj = project_partial(value_partial, value_basis)
+    out_part, value_part = local_grads(
+        query_rows, key_rows, value_rows, mix_lambda, head_gain, out_cotangent, layer_input,
+        value_cotangent, out_basis, value_basis,
+    )
+    out_proj = lax.psum_scatter(out_part, "fs", scatter_dimension=0, tiled=True)
+    value_proj = lax.psum_scatter(value_part, "fs", scatter_dimension=0, tiled=True)
     new_out_first, new_out_second, out_dir = moment_step(out_proj, out_first, out_second)
     new_value_first, new_value_second, value_dir = moment_step(
         value_proj, value_first, value_second

time: 580 us -> 405 us (0.70)
  matrix products: 146 us -> 5 us
  other arithmetic: 102 us -> 4.24 us
  Pallas kernels: 0 us -> 75.4 us
  local copies, waits for them, and re-layouts: 25.2 us -> 6.04 us
  waiting for transfers between devices: 183 us -> 195 us
    div x4 -> x0, other arithmetic: 94.9 us -> none  [one_block(): soft_maps = exp_scores / jnp.sum(exp_scores, axis=-1, keepdims=True)]
    pallas_call x0 -> x1, Pallas kernels: none -> 75.4 us  [local_grads(): pl.pallas_call(grads_kernel, grid=(blocks, heads), out_shape=(jax.ShapeDt...]
    sub x4 -> x0, matrix products: 71.7 us -> none  [one_block(): exp_scores = jnp.exp(scores - row_peak)]
    dot_general x8 -> x0, matrix products: 69.5 us -> none  [the longest x4 49.2 us: one_block(): jnp.einsum('hqk,khv->qhv', mix_weights, value_three, preferred_element_ty...]
    unnamed x29 -> x16, local copies, waits for them, and re-layouts: 18.7 us -> 4.65 us
    reduce_scatter x2, waiting for transfers between devices: 117 us -> 128 us  [the longest x1 64.6 us: body(): lax.psum_scatter(value_part, 'fs', scatter_dimension=0, tiled=True)]
  transfers between devices with their start and end apart: 4 -> 4, of which waited for: 4 -> 4; matrix products, arithmetic and copies ran while one was open for 3% -> 1% of each run, Pallas kernels for 0% -> 0%
where the time goes in v1:
time: 405 us
  waiting for transfers between devices  195 us (48%)
  blocking collectives  104 us (26%)
  Pallas kernels  75.4 us (19%)
  between operations  15.2 us (4%)
  local copies, waits for them, and re-layouts  6.04 us (1%)
  matrix products  5 us (1%)
  other arithmetic  4.24 us (1%)
    pallas_call x1, Pallas kernels, local_grads(): pl.pallas_call(grads_kernel, grid=(blocks, heads), out_shape=(jax.ShapeDt...  75.4 us
    reduce_scatter x1, waiting for transfers between devices, body(): lax.psum_scatter(value_part, 'fs', scatter_dimension=0, tiled=True)  64.6 us
    reduce_scatter x1, waiting for transfers between devices, body(): out_proj = lax.psum_scatter(out_part, 'fs', scatter_dimension=0, tiled=True)  63.4 us
    all_gather x1, waiting for transfers between devices, body(): lax.all_gather(new_out_weight.astype(jnp.bfloat16), 'fs', axis=1, tiled=T...  51.9 us
    psum x1, blocking collectives, body(): lax.psum((jnp.sum(out_dir * out_dir), jnp.sum(value_dir * value_dir)), ('...  40.2 us
    all_gather x1, blocking collectives, body(): lax.all_gather(out_dir, 'fs', axis=0, tiled=True)  32.5 us
    all_gather x1, blocking collectives, body(): lax.all_gather(value_dir, 'fs', axis=0, tiled=True)  31.3 us
    all_gather x1, waiting for transfers between devices, body(): lax.all_gather(new_value_weight.astype(jnp.bfloat16), 'fs', axis=0, tiled...  13.9 us
  transfers between devices with their start and end apart: 4, of which 4 were waited for; matrix products, arithmetic and copies ran while one was open for 1% of the time, Pallas kernels for 0%

profile of v1, /device:TPU:0, one launch (start us, length us, event | category | flops | bytes accessed | tf_op | source)
XLA Modules:
  0.0 404.6 jit_solution(13733997696671738056)
XLA Ops:
  7.2 0.0 reduce-scatter.5.cloned.1.call-start
  7.2 1.4 copy.26.gain_ref
  8.6 75.4 %grads.1 = (f32[256,512]{1,0:T(8,128)}, f32[256,512]{1,0:T(8,128)}) custom-call(f32[4]{0:T(128)} %lam_ref.1, bf16[2048,512]{1,0:T(8,128)(2,1)} %query_ref.1, bf16[2048,512]{1,0:T(8,128)(2,1)} %key_ref.1, bf16[2048,512]{1,0:T(8,128)(2,1)} %value_ref.1, f32[128,1]{1,0:T(8,128)} %copy.26.gain_ref, bf16[2048,2048]{1,0:T(8,128)(2,1)} %cot_ref.1, ...), custom_call_target="tpu_custom_call" | custom-call | tf_op jit(solution)/shard_map/grads/pallas_call | solution.py:143
  84.0 0.0 reduce-scatter.5.cloned.1.call-update
  84.0 0.0 reduce-scatter.3.cloned.1.call-start
  84.1 0.7 reduce-scatter.3.cloned.1.call-update
  84.8 0.0 all-gather.5.cloned.1.call-start
  84.8 64.6 %reduce-scatter.5.cloned.1.call-done = f32[32,512]{1,0:T(8,128)} async-done(((f32[256,512]{1,0:T(8,128)}), f32[32,512]{1,0:T(8,128)}) %reduce-scatter.5.cloned.1.call-update) | async-done | bytes 65552 | tf_op jit(solution)/shard_map/reduce_scatter | solution.py:219
  149.4 0.0 copy-done.3
  149.4 2.1 multiply_reduce_fusion
  151.6 63.4 %reduce-scatter.3.cloned.1.call-done = f32[32,512]{1,0:T(8,128)} async-done(((f32[256,512]{1,0:T(8,128)}), f32[32,512]{1,0:T(8,128)}) %reduce-scatter.3.cloned.1.call-update) | async-done | bytes 65552 | tf_op jit(solution)/shard_map/reduce_scatter | solution.py:218
  215.0 2.1 multiply_reduce_fusion.1
  217.1 40.2 %all-reduce = (f32[]{:T(128)}, f32[]{:T(128)}) all-reduce(f32[]{:T(128)} %get-tuple-element.24, f32[]{:T(128)} %get-tuple-element.20), channel_id=1, replica_groups=mesh['fs'=8,'tp'=4] {'fs','tp'}, use_global_device_ids=true, to_apply=%region_2.0 | all-reduce | flops 2 | bytes 16 | tf_op jit(solution)/shard_map/psum | solution.py:224
  258.0 31.3 %all_gather.13 = f32[256,512]{1,0:T(8,128)S(1)} all-gather(f32[32,512]{1,0:T(8,128)S(1)} %get-tuple-element.21), channel_id=1, replica_groups=mesh['fs'=8,'tp'=4] {'fs'}, dimensions={0}, use_global_device_ids=true | all-gather | bytes 589824 | tf_op jit(solution)/shard_map/all_gather | solution.py:237
  289.3 2.4 fusion.6
  291.8 0.0 all-gather.5.cloned.1.call-update
  291.8 0.0 all-gather.3.cloned.1.call-start
  292.5 32.5 %all_gather.12 = f32[256,512]{1,0:T(8,128)S(1)} all-gather(f32[32,512]{1,0:T(8,128)S(1)} %get-tuple-element.25), channel_id=1, replica_groups=mesh['fs'=8,'tp'=4] {'fs'}, dimensions={0}, use_global_device_ids=true | all-gather | bytes 589824 | tf_op jit(solution)/shard_map/all_gather | solution.py:232
  325.0 2.6 fusion.7
  327.6 0.0 all-gather.3.cloned.1.call-update
  327.6 13.9 %all-gather.5.cloned.1.call-done = bf16[2048,512]{1,0:T(8,128)(2,1)} async-done(((bf16[256,512]{1,0:T(8,128)(2,1)}), bf16[2048,512]{1,0:T(8,128)(2,1)}) %all-gather.5.cloned.1.call-update) | async-done | bytes 2097168 | tf_op jit(solution)/shard_map/all_gather | solution.py:246
  341.6 51.9 %all-gather.3.cloned.1.call-done = bf16[512,2048]{1,0:T(8,128)(2,1)} async-done(((bf16[512,256]{1,0:T(8,128)(2,1)}), bf16[512,2048]{1,0:T(8,128)(2,1)}) %all-gather.3.cloned.1.call-update) | async-done | bytes 2097168 | tf_op jit(solution)/shard_map/all_gather | solution.py:245
  393.5 3.3 copy.29
  396.8 1.3 copy.30
  (13 shorter events, 0.0 us)
Async XLA Ops:
  7.2 142.3 %reduce-scatter.5.cloned.1.call-start = ((), (), s32[]{:S(2)}) async-start(), calls=%async_computation.3 | async-start | bytes 589824 | tf_op jit(solution)/shard_map/reduce_scatter | solution.py:219
  8.6 140.8 %copy-start.3 = (f32[32,512]{1,0:T(8,128)S(1)}, f32[32,512]{1,0:T(8,128)}, u32[]{:S(2)}) copy-start(f32[32,512]{1,0:T(8,128)} %param.31) | copy-start | bytes 196612
  8.6 140.8 %copy-start.4 = (f32[32,512]{1,0:T(8,128)S(1)}, f32[32,512]{1,0:T(8,128)}, u32[]{:S(2)}) copy-start(f32[32,512]{1,0:T(8,128)} %param.30) | copy-start | bytes 196612
  8.6 206.4 %copy-start.5 = (f32[32,512]{1,0:T(8,128)S(1)}, f32[32,512]{1,0:T(8,128)}, u32[]{:S(2)}) copy-start(f32[32,512]{1,0:T(8,128)} %param.29) | copy-start | bytes 196612
  8.6 206.4 %copy-start.6 = (f32[32,512]{1,0:T(8,128)S(1)}, f32[32,512]{1,0:T(8,128)}, u32[]{:S(2)}) copy-start(f32[32,512]{1,0:T(8,128)} %param.28) | copy-start | bytes 196612
  84.0 205.4 %copy-start.1 = (f32[256,512]{1,0:T(8,128)S(1)}, f32[256,512]{1,0:T(8,128)}, u32[]{:S(2)}) copy-start(f32[256,512]{1,0:T(8,128)} %param.25) | copy-start | bytes 1572868
  84.0 131.0 %reduce-scatter.3.cloned.1.call-start = ((), (), s32[]{:S(2)}) async-start(), calls=%async_computation.2 | async-start | bytes 589824 | tf_op jit(solution)/shard_map/reduce_scatter | solution.py:218
  84.8 256.8 %all-gather.5.cloned.1.call-start = ((), (), s32[]{:S(2)}) async-start(), calls=%async_computation.5 | async-start | bytes 2359296 | tf_op jit(solution)/shard_map/all_gather | solution.py:246
  151.6 173.5 %copy-start.2 = (f32[512,256]{1,0:T(8,128)S(1)}, f32[512,256]{1,0:T(8,128)}, u32[]{:S(2)}) copy-start(f32[512,256]{1,0:T(8,128)} %param.24) | copy-start | bytes 1572868
  291.8 101.7 %all-gather.3.cloned.1.call-start = ((), (), s32[]{:S(2)}) async-start(), calls=%async_computation.4 | async-start | bytes 2359296 | tf_op jit(solution)/shard_map/all_gather | solution.py:245
  393.5 3.3 copy-start
Sparse Core Ops, SparseCore 0:
  84.1 65.2 reduce-scatter.4
  153.4 61.5 reduce-scatter.2
  291.9 49.5 all-gather.4
  344.0 49.3 all-gather.2

commit v2 on v1

--- a/solution.py
+++ b/solution.py
@@ -188,74 +188,263 @@
     return (new_first, new_second, direction)
 
 
-def body(
-    query_rows,
-    key_rows,
-    value_rows,
-    mix_lambda,
-    head_gain,
-    out_cotangent,
-    layer_input,
-    value_cotangent,
-    out_weight,
-    value_weight,
-    out_basis,
-    value_basis,
-    out_first,
-    out_second,
-    value_first,
-    value_second,
+def finish_kernel(
+    fs_count, tp_count,
+    opart, vpart, ofirst, osecond, vfirst, vsecond, obasis, vbasis, oweight, vweight,
+    ostep, vstep, onew, vnew, ocopy, vcopy, ofirst_new, osecond_new, vfirst_new, vsecond_new,
+    got, dirs, squares, squares_got,
+    scatter_send, scatter_recv, ring_send, ring_recv, copy_send, copy_recv, sq_send, sq_recv,
+):
+    me = lax.axis_index("fs")
+    my_tp = lax.axis_index("tp")
+    half_count = fs_count // 2
+    rank_share = ofirst.shape[0]
+    cols = ofirst.shape[1]
+    row_share = vweight.shape[0]
+    mesh_ids = pl.DeviceIdType.MESH
+
+    place = jnp.where(me % 2 == 0, me // 2, fs_count - 1 - me // 2)
+
+    def owner(at):
+        at = lax.rem(at + 2 * fs_count, fs_count)
+        return jnp.where(at < half_count, 2 * at, 2 * (fs_count - 1 - at) + 1)
+
+    def fs_peer(gap):
+        return lax.rem(me + gap, fs_count)
+
+    def tp_peer(gap):
+        return lax.rem(my_tp + gap, tp_count)
+
+    barrier = pltpu.get_barrier_semaphore()
+    for gap in range(1, fs_count):
+        pl.semaphore_signal(
+            barrier, inc=1, device_id=(fs_peer(gap), my_tp), device_id_type=mesh_ids
+        )
+    for gap in range(1, tp_count):
+        pl.semaphore_signal(
+            barrier, inc=1, device_id=(me, tp_peer(gap)), device_id_type=mesh_ids
+        )
+    pl.semaphore_wait(barrier, fs_count + tp_count - 2)
+
+    def share(index, size):
+        return pl.ds(pl.multiple_of(index * size, size), size)
+
+    parts = (vpart, opart)
+    scatters = ([], [])
+    for mat in range(2):
+        for gap in range(1, fs_count):
+            peer = fs_peer(gap)
+            copy = pltpu.make_async_remote_copy(
+                src_ref=parts[mat].at[share(peer, rank_share)],
+                dst_ref=got.at[mat, gap - 1],
+                send_sem=scatter_send.at[mat, gap - 1],
+                recv_sem=scatter_recv.at[mat, gap - 1],
+                device_id=(peer, my_tp),
+                device_id_type=mesh_ids,
+            )
+            copy.start()
+            scatters[mat].append(copy)
+
+    def ring(blocks, sems_send, sems_recv):
+        def make(mat, step, way):
+            origin = owner(place - step if way == 0 else place + step)
+            split = way if step == half_count - 1 else None
+            ref = blocks[mat](origin, split)
+            target = owner(place + 1 if way == 0 else place - 1)
+            return pltpu.make_async_remote_copy(
+                src_ref=ref,
+                dst_ref=ref,
+                send_sem=sems_send.at[mat, way, step],
+                recv_sem=sems_recv.at[mat, way, step],
+                device_id=(target, my_tp),
+                device_id_type=mesh_ids,
+            )
+
+        def arrival(mat, step, way):
+            origin = owner(place - 1 - step if way == 0 else place + 1 + step)
+            split = way if step == half_count - 1 else None
+            ref = blocks[mat](origin, split)
+            return pltpu.make_async_remote_copy(
+                src_ref=ref,
+                dst_ref=ref,
+                send_sem=sems_send.at[mat, way, step],
+                recv_sem=sems_recv.at[mat, way, step],
+                device_id=(owner(place + 1), my_tp),
+                device_id_type=mesh_ids,
+            )
+
+        started = []
+
+        def begin(mat):
+            for way in range(2):
+                copy = make(mat, 0, way)
+                copy.start()
+                started.append(copy)
+
+        def drain():
+            for step in range(half_count):
+                for mat in range(len(blocks)):
+                    for way in range(2):
+                        arrival(mat, step, way).wait_recv()
+                        if step + 1 < half_count:
+                            copy = make(mat, step + 1, way)
+                            copy.start()
+                            started.append(copy)
+            for copy in started:
+                copy.wait_send()
+
+        return begin, drain
+
+    def halved(start, size, split):
+        if split is None:
+            return pl.ds(pl.multiple_of(start, size), size)
+        return pl.ds(pl.multiple_of(start + split * (size // 2), size // 2), size // 2)
+
+    begin, drain = ring(
+        [
+            lambda at, split, mat=mat: dirs.at[mat, halved(at * rank_share, rank_share, split)]
+            for mat in range(2)
+        ],
+        ring_send, ring_recv,
+    )
+    moments = (
+        (vfirst, vsecond, vfirst_new, vsecond_new),
+        (ofirst, osecond, ofirst_new, osecond_new),
+    )
+    for mat in range(2):
+        proj = parts[mat][share(me, rank_share), :]
+        for gap in range(1, fs_count):
+            scatters[mat][gap - 1].wait_recv()
+            proj += got[mat, gap - 1]
+        first, second, first_new, second_new = moments[mat]
+        new_first, new_second, direction = moment_step(proj, first[...], second[...])
+        dirs[mat, share(me, rank_share), :] = direction
+        begin(mat)
+        first_new[...] = new_first
+        second_new[...] = new_second
+    drain()
+
+    for mat in range(2):
+        whole = dirs[mat]
+        squared = fold_rows(whole * whole, jnp.sum)
+        total = squared[:, :128]
+        for at in range(128, cols, 128):
+            total += squared[:, at : at + 128]
+        squares[mat] = total
+    exchanges = []
+    for gap in range(1, tp_count):
+        copy = pltpu.make_async_remote_copy(
+            src_ref=squares,
+            dst_ref=squares_got.at[gap - 1],
+            send_sem=sq_send.at[gap - 1],
+            recv_sem=sq_recv.at[gap - 1],
+            device_id=(me, tp_peer(gap)),
+            device_id_type=mesh_ids,
+        )
+        copy.start()
+        exchanges.append(copy)
+
+    high, low = split_two(dirs[0])
+    vstep[...] = dot_f32(vbasis[...], high) + dot_f32(vbasis[...], low)
+    high, low = split_two(dirs[1])
+    ostep[...] = dot_f32(high, obasis[...], ((0,), (1,))) + dot_f32(
+        low, obasis[...], ((0,), (1,))
+    )
+    for copy in exchanges:
+        copy.wait_recv()
+    entry_count = rank_share * fs_count * cols * tp_count
+
+    def clip_of(mat):
+        total = squares[mat]
+        for gap in range(1, tp_count):
+            total += squares_got[gap - 1, mat]
+        total = jnp.sum(jnp.sum(total, axis=0, keepdims=True), axis=1, keepdims=True)
+        return jnp.minimum(1.0, CLIP_RMS * math.sqrt(entry_count) / jnp.sqrt(total))
+
+    begin, drain = ring(
+        [
+            lambda at, split: vcopy.at[halved(at * row_share, row_share, split)],
+            lambda at, split: ocopy.at[
+                slice(None) if split is None else pl.ds(split * (cols // 2), cols // 2),
+                share(at, row_share),
+            ],
+        ],
+        copy_send, copy_recv,
+    )
+    step = clip_of(0) * vstep[...]
+    vstep[...] = step
+    weight = vweight[...] - LEARN_RATE * step
+    vnew[...] = weight
+    vcopy[share(me, row_share), :] = weight.astype(BF16)
+    begin(0)
+    step = clip_of(1) * ostep[...]
+    ostep[...] = step
+    weight = oweight[...] - LEARN_RATE * step
+    onew[...] = weight
+    ocopy[:, share(me, row_share)] = weight.astype(BF16)
+    begin(1)
+    drain()
+    for copy in scatters[0] + scatters[1] + exchanges:
+        copy.wait_send()
+
+
+def finish(
+    out_part, value_part, out_first, out_second, value_first, value_second, out_rows_b,
+    value_rows_b, out_weight, value_weight,
 ):
     fs_count = lax.axis_size("fs")
-    row_share = out_cotangent.shape[1] // fs_count
+    tp_count = lax.axis_size("tp")
+    rank, cols = out_part.shape
+    row_share = value_weight.shape[0]
+    like = lambda a: jax.ShapeDtypeStruct(a.shape, a.dtype)
+    half_count = fs_count // 2
+    dma = pltpu.SemaphoreType.DMA
+    return pl.pallas_call(
+        functools.partial(finish_kernel, fs_count, tp_count),
+        out_shape=(
+            like(out_weight), like(value_weight), like(out_weight), like(value_weight),
+            jax.ShapeDtypeStruct((cols, row_share * fs_count), BF16),
+            jax.ShapeDtypeStruct((row_share * fs_count, cols), BF16),
+            like(out_first), like(out_second), like(value_first), like(value_second),
+        ),
+        in_specs=[pl.BlockSpec(memory_space=pltpu.VMEM)] * 10,
+        out_specs=tuple([pl.BlockSpec(memory_space=pltpu.VMEM)] * 10),
+        scratch_shapes=[
+            pltpu.VMEM((2, fs_count - 1, rank // fs_count, cols), F32),
+            pltpu.VMEM((2, rank, cols), F32),
+            pltpu.VMEM((2, 8, 128), F32),
+            pltpu.VMEM((tp_count - 1, 2, 8, 128), F32),
+            dma((2, fs_count - 1)), dma((2, fs_count - 1)),
+            dma((2, 2, half_count)), dma((2, 2, half_count)),
+            dma((2, 2, half_count)), dma((2, 2, half_count)),
+            dma((tp_count - 1,)), dma((tp_count - 1,)),
+        ],
+        compiler_params=pltpu.CompilerParams(
+            collective_id=0, has_side_effects=True, vmem_limit_bytes=48 * 1024 * 1024
+        ),
+        name="finish",
+    )(
+        out_part, value_part, out_first, out_second, value_first, value_second, out_rows_b,
+        value_rows_b, out_weight, value_weight,
+    )
+
+
+def body(
+    query_rows, key_rows, value_rows, mix_lambda, head_gain, out_cotangent, layer_input,
+    value_cotangent, out_weight, value_weight, out_basis, value_basis, out_first, out_second,
+    value_first, value_second,
+):
+    row_share = out_cotangent.shape[1] // lax.axis_size("fs")
     row_base = lax.axis_index("fs") * row_share
-    out_rows_b = lax.dynamic_slice_in_dim(out_basis, row_base, row_share, 0).astype(jnp.float32)
-    value_rows_b = lax.dynamic_slice_in_dim(value_basis, row_base, row_share, 0).astype(jnp.float32)
+    out_rows_b = lax.dynamic_slice_in_dim(out_basis, row_base, row_share, 0)
+    value_rows_b = lax.dynamic_slice_in_dim(value_basis, row_base, row_share, 0)
     out_part, value_part = local_grads(
         query_rows, key_rows, value_rows, mix_lambda, head_gain, out_cotangent, layer_input,
         value_cotangent, out_basis, value_basis,
     )
-    out_proj = lax.psum_scatter(out_part, "fs", scatter_dimension=0, tiled=True)
-    value_proj = lax.psum_scatter(value_part, "fs", scatter_dimension=0, tiled=True)
-    new_out_first, new_out_second, out_dir = moment_step(out_proj, out_first, out_second)
-    new_value_first, new_value_second, value_dir = moment_step(
-        value_proj, value_first, value_second
-    )
-    out_sumsq, value_sumsq = lax.psum(
-        (jnp.sum(out_dir * out_dir), jnp.sum(value_dir * value_dir)), ("fs", "tp")
-    )
-    entry_count = out_first.shape[0] * fs_count * out_first.shape[1] * lax.axis_size("tp")
-    out_clip = jnp.minimum(1.0, CLIP_RMS * math.sqrt(entry_count) / jnp.sqrt(out_sumsq))
-    value_clip = jnp.minimum(1.0, CLIP_RMS * math.sqrt(entry_count) / jnp.sqrt(value_sumsq))
-    out_total = jnp.dot(
-        out_rows_b,
-        lax.all_gather(out_dir, "fs", axis=0, tiled=True),
-        precision=lax.Precision.HIGHEST,
-    )
-    value_total = jnp.dot(
-        value_rows_b,
-        lax.all_gather(value_dir, "fs", axis=0, tiled=True),
-        precision=lax.Precision.HIGHEST,
-    )
-    value_step = value_clip * value_total
-    out_step = (out_clip * out_total).T
-    new_value_weight = value_weight - LEARN_RATE * value_step
-    new_out_weight = out_weight - LEARN_RATE * out_step
-    out_copy, value_copy = (
-        lax.all_gather(new_out_weight.astype(jnp.bfloat16), "fs", axis=1, tiled=True),
-        lax.all_gather(new_value_weight.astype(jnp.bfloat16), "fs", axis=0, tiled=True),
-    )
-    return (
-        out_step,
-        value_step,
-        new_out_weight,
-        new_value_weight,
-        out_copy,
-        value_copy,
-        new_out_first,
-        new_out_second,
-        new_value_first,
-        new_value_second,
+    return finish(
+        out_part, value_part, out_first, out_second, value_first, value_second, out_rows_b,
+        value_rows_b, out_weight, value_weight,
     )
 
 

time: 405 us -> 182 us (0.45)
  waiting for transfers between devices: 195 us -> 0 us
  blocking collectives: 104 us -> 0 us
  Pallas kernels: 75.4 us -> 167 us
  between operations: 15.2 us -> 0.77 us
  local copies, waits for them, and re-layouts: 6.04 us -> 13.9 us
  matrix products: 5 us -> 0 us
  other arithmetic: 4.24 us -> 0 us
    reduce_scatter x2 -> x0, waiting for transfers between devices: 128 us -> none  [the longest x1 64.6 us: body(): lax.psum_scatter(value_part, 'fs', scatter_dimension=0, tiled=True)]
    pallas_call x0 -> x1, Pallas kernels: none -> 91.7 us  [finish(): pl.pallas_call(functools.partial(finish_kernel, fs_count, tp_count), out_...]
    all_gather x2 -> x0, waiting for transfers between devices: 65.8 us -> none  [the longest x1 51.9 us: body(): lax.all_gather(new_out_weight.astype(jnp.bfloat16), 'fs', axis=1, tiled=T...]
    all_gather x2 -> x0, blocking collectives: 63.8 us -> none  [the longest x1 32.5 us: body(): lax.all_gather(out_dir, 'fs', axis=0, tiled=True)]
    psum x1 -> x0, blocking collectives: 40.2 us -> none  [body(): lax.psum((jnp.sum(out_dir * out_dir), jnp.sum(value_dir * value_dir)), ('...]
    unnamed x16 -> x30, local copies, waits for them, and re-layouts: 4.65 us -> 11.5 us
    dot_general x2 -> x0, matrix products: 5 us -> none  [the longest x1 2.57 us: body(): jnp.dot(out_rows_b, lax.all_gather(out_dir, 'fs', axis=0, tiled=True), pr...]
    reduce_sum x2 -> x0, other arithmetic: 4.24 us -> none  [the longest x1 2.12 us: body(): jnp.sum(value_dir * value_dir)]
  transfers between devices with their start and end apart: 4 -> 0, of which waited for: 4 -> 0; matrix products, arithmetic and copies ran while one was open for 1% -> 0% of each run, Pallas kernels for 0% -> 0%
where the time goes in v2:
time: 182 us
  Pallas kernels  167 us (92%)
  local copies, waits for them, and re-layouts  13.9 us (8%)
    pallas_call x1, Pallas kernels, finish(): pl.pallas_call(functools.partial(finish_kernel, fs_count, tp_count), out_...  91.7 us
    pallas_call x1, Pallas kernels, local_grads(): pl.pallas_call(grads_kernel, grid=(blocks, heads), out_shape=(jax.ShapeDt...  75.3 us
    unnamed x30, local copies, waits for them, and re-layouts  11.5 us

profile of v2, /device:TPU:0, one launch (start us, length us, event | category | flops | bytes accessed | tf_op | source)
XLA Modules:
  0.0 181.6 jit_solution(16358269975436792741)
XLA Ops:
  0.6 1.4 copy.26.gain_ref
  2.0 1.0 constant_dynamic-slice_fusion
  3.0 0.0 copy-start
  3.0 0.0 copy-start.1
  3.0 0.0 copy-start.4
  3.1 0.0 copy-start.5
  3.1 0.0 copy-start.6
  3.1 0.0 copy-start.7
  3.1 75.3 %grads.1 = (f32[256,512]{1,0:T(8,128)}, f32[256,512]{1,0:T(8,128)}) custom-call(f32[4]{0:T(128)} %lam_ref.1, bf16[2048,512]{1,0:T(8,128)(2,1)} %query_ref.1, bf16[2048,512]{1,0:T(8,128)(2,1)} %key_ref.1, bf16[2048,512]{1,0:T(8,128)(2,1)} %value_ref.1, f32[128,1]{1,0:T(8,128)} %copy.26.gain_ref, bf16[2048,2048]{1,0:T(8,128)(2,1)} %cot_ref.1, ...), custom_call_target="tpu_custom_call" | custom-call | tf_op jit(solution)/shard_map/grads/pallas_call | solution.py:143
  78.5 0.0 copy-start.2
  78.5 1.0 copy-done.2
  79.5 1.0 copy-done.3
  80.6 91.7 %finish.1 = (f32[512,256]{1,0:T(8,128)S(1)}, f32[256,512]{1,0:T(8,128)S(1)}, f32[512,256]{1,0:T(8,128)S(1)}, f32[256,512]{1,0:T(8,128)S(1)}, bf16[512,2048]{1,0:...) custom-call(f32[256,512]{1,0:T(8,128)S(1)} %copy-done.2, ...), custom_call_target="tpu_custom_call" | custom-call | tf_op jit(solution)/shard_map/finish/pallas_call | solution.py:402
  172.3 0.8 copy.37
  173.1 0.8 copy.38
  173.9 0.8 copy.39
  174.6 0.8 copy.40
  175.4 1.3 copy.41
  176.8 1.0 copy-done.8
  177.8 1.3 copy.42
  179.1 0.6 copy.43
  179.7 0.6 copy.44
  180.4 0.6 copy.45
  181.0 0.6 copy.46
  (10 shorter events, 0.0 us)
Async XLA Ops:
  3.0 75.4 %copy-start = (f32[512,256]{1,0:T(8,128)S(1)}, f32[512,256]{1,0:T(8,128)}, u32[]{:S(2)}) copy-start(f32[512,256]{1,0:T(8,128)} %oweight.1) | copy-start | bytes 1572868
  3.0 75.4 %copy-start.1 = (f32[256,512]{1,0:T(8,128)S(1)}, f32[256,512]{1,0:T(8,128)}, u32[]{:S(2)}) copy-start(f32[256,512]{1,0:T(8,128)} %vweight.1) | copy-start | bytes 1572868
  3.0 75.4 %copy-start.4 = (f32[32,512]{1,0:T(8,128)S(1)}, f32[32,512]{1,0:T(8,128)}, u32[]{:S(2)}) copy-start(f32[32,512]{1,0:T(8,128)} %ofirst.1) | copy-start | bytes 196612
  3.1 75.4 %copy-start.5 = (f32[32,512]{1,0:T(8,128)S(1)}, f32[32,512]{1,0:T(8,128)}, u32[]{:S(2)}) copy-start(f32[32,512]{1,0:T(8,128)} %osecond.1) | copy-start | bytes 196612
  3.1 75.4 %copy-start.6 = (f32[32,512]{1,0:T(8,128)S(1)}, f32[32,512]{1,0:T(8,128)}, u32[]{:S(2)}) copy-start(f32[32,512]{1,0:T(8,128)} %vfirst.1) | copy-start | bytes 196612
  3.1 75.4 %copy-start.7 = (f32[32,512]{1,0:T(8,128)S(1)}, f32[32,512]{1,0:T(8,128)}, u32[]{:S(2)}) copy-start(f32[32,512]{1,0:T(8,128)} %vsecond.1) | copy-start | bytes 196612
  78.5 1.0 copy-start.2
  79.5 1.0 copy-start.3
  172.3 3.2 %copy-start.9 = (bf16[512,2048]{1,0:T(8,128)(2,1)S(1)}, bf16[512,2048]{1,0:T(8,128)(2,1)}, u32[]{:S(2)}) copy-start(bf16[512,2048]{1,0:T(8,128)(2,1)} %get-tuple-element.30) | copy-start | bytes 6291460
  175.4 2.3 %copy-start.8 = (bf16[2048,512]{1,0:T(8,128)(2,1)S(1)}, bf16[2048,512]{1,0:T(8,128)(2,1)}, u32[]{:S(2)}) copy-start(bf16[2048,512]{1,0:T(8,128)(2,1)} %get-tuple-element.31) | copy-start | bytes 6291460
